TPU v7x, 512 devices: a whole 4x4x16 slice. The times are simulated.
512 devices in a mesh: ep: 32 (over z, core), tp: 16 (over y, x).
Axes of the slice: x: 4, y: 4, z: 16, core: 2. Of those that a mesh axis runs over, the one named last changes fastest.
Arguments:
- query_rows: bfloat16 [24576, 1024], P('ep', 'tp'), may hold values from -600 to 600
- key_rows: bfloat16 [24576, 1024], P('ep', 'tp'), may hold values from -6 to 6
- value_rows: bfloat16 [24576, 1024], P('ep', 'tp'), may hold values from -6 to 6
- cum_gate: float32 [16, 24576], P('tp'), may hold values from -2458 to 0, as said below
- out_weight: bfloat16 [1024, 2048], P(None, 'tp'), may hold values from -0.1875 to 0.1875
- moe_input: bfloat16 [6144, 2048], P('ep'), may hold values from -6 to 6
- moe_gain: float32 [2048], replicated, may hold values from 0.1 to 1.9
- routes: int32 [6144, 3], P('ep'), may hold values from 0 to 127, all different within a row; in each aligned block of 192 rows (0 to 191, 192 to 383, ...) at most 9 rows name the same one
- route_weight: float32 [6144, 3], P('ep'), may hold values from 0.2 to 1.5
- expert_gate: bfloat16 [128, 2048, 512], P('ep', None, 'tp'), may hold values from -0.125 to 0.125
- expert_up: bfloat16 [128, 2048, 512], P('ep', None, 'tp'), may hold values from -0.125 to 0.125
- expert_down: bfloat16 [128, 512, 2048], P('ep', None, 'tp'), may hold values from -0.25 to 0.25
- shared_gate: bfloat16 [2048, 512], P(None, 'tp'), may hold values from -0.125 to 0.125
- shared_up: bfloat16 [2048, 512], P(None, 'tp'), may hold values from -0.125 to 0.125
- shared_down: bfloat16 [512, 2048], P(None, 'tp'), may hold values from -0.25 to 0.25
Outputs:
- mixer_out: bfloat16 [24576, 2048], P('ep', 'tp')
- moe_out: bfloat16 [6144, 2048], P('ep', 'tp')
Inputs may be any that keep to these rules, and one draw needn't show every extreme that they name: Non-increasing along positions: cum_gate[h, t] is the sum of the log forget gates of head h over positions 0 to t. `routes`: the 3 experts of a token differ. In each aligned block of 192 tokens no expert is named by more than 9 tokens, a bound that some block reaches.
All inputs are finite; a program needn't handle non-finite values.
Results may differ from a plain program's by a relative error of at most 0.0068.
Values may be sent and summed in bfloat16 or wider, within the bound.
A program may use at most 64 MiB of HBM per device.

v0:
```python
import jax
import jax.numpy as jnp
from jax import lax
from jax.sharding import PartitionSpec as P

HEAD = 64


neg_fill = -1e30
norm_eps = 1e-06


def joined_along(pieces, dim):
    dims = list(pieces.shape[1:])
    dims[dim] *= pieces.shape[0]
    return jnp.moveaxis(pieces, 0, dim).reshape(dims)


def sent_to_all(array, axis):
    copies = jnp.broadcast_to(array, (lax.axis_size(axis), *array.shape))
    return lax.all_to_all(copies, axis, split_axis=0, concat_axis=0, tiled=True)


def collect(array, axis, dim):
    return joined_along(sent_to_all(array, axis), dim)


def local(
    query_rows,
    key_rows,
    value_rows,
    cum_gate,
    out_weight,
    moe_input,
    moe_gain,
    routes,
    route_weight,
    expert_gate,
    expert_up,
    expert_down,
    shared_gate,
    shared_up,
    shared_down,
):
    row_count = query_rows.shape[0]
    width = query_rows.shape[1]
    local_heads = width // HEAD
    scale = HEAD ** (-0.5)
    first_row = lax.axis_index("ep") * row_count
    last_row = first_row + row_count - 1
    query_heads = query_rows.reshape(row_count, local_heads, HEAD)
    query_gate = lax.dynamic_slice_in_dim(cum_gate, first_row, row_count, 1)
    query_pos = first_row + jnp.arange(row_count, dtype=jnp.int32)
    key_value = jnp.concatenate([key_rows, value_rows], axis=1)
    initial = (
        jnp.full((local_heads, row_count), neg_fill, jnp.float32),
        jnp.zeros((local_heads, row_count), jnp.float32),
        jnp.zeros((local_heads, row_count, HEAD), jnp.float32),
    )
    shard_rows = lax.all_gather(key_value, "ep", axis=0, tiled=True)
    piece_len = shard_rows.shape[0]
    key_span = 512

    def one_span(state_in, span_index):
        span_start = span_index * key_span

        def update(state_old):
            running_max, denominator, weighted = state_old
            block = lax.dynamic_slice_in_dim(shard_rows, span_index * key_span, key_span, 0)
            keys_block = block[:, :width].reshape(key_span, local_heads, HEAD)
            values_block = block[:, width:].reshape(key_span, local_heads, HEAD)
            key_gate = lax.dynamic_slice_in_dim(cum_gate, span_start, key_span, 1)
            scores = (
                jnp.einsum(
                    "qhd,khd->hqk", query_heads, keys_block, preferred_element_type=jnp.float32
                )
                * scale
            )
            scores = scores + query_gate[:, :, None] - key_gate[:, None, :]
            causal = (span_start + jnp.arange(key_span, dtype=jnp.int32))[None, :] <= query_pos[
                :, None
            ]
            scores = jnp.where(causal[None], scores, neg_fill)
            new_max = jnp.maximum(running_max, jnp.max(scores, axis=2))
            expon = jnp.where(causal[None], jnp.exp(scores - new_max[:, :, None]), 0.0)
            rescale = jnp.exp(running_max - new_max)
            denominator = denominator * rescale + jnp.sum(expon, axis=2)
            weighted = weighted * rescale[:, :, None] + jnp.einsum(
                "hqk,khd->hqd",
                expon.astype(jnp.bfloat16),
                values_block,
                preferred_element_type=jnp.float32,
            )
            return (new_max, denominator, weighted)

        state_next = lax.cond(span_start <= last_row, update, lambda unchanged: unchanged, state_in)
        return (state_next, None)

    state_out, _ = lax.scan(one_span, initial, jnp.arange(piece_len // key_span, dtype=jnp.int32))
    running_max, denominator, weighted = state_out
    heads_out = (weighted / denominator[:, :, None]).transpose(1, 0, 2).reshape(row_count, width)
    heads_out = heads_out.astype(jnp.bfloat16)
    token_count = moe_input.shape[0]
    top_count = routes.shape[1]
    local_experts = expert_gate.shape[0]
    ep_count = lax.axis_size("ep")
    expert_count = local_experts * ep_count
    capacity = 2 * token_count * top_count // expert_count
    column_count = expert_down.shape[2]
    first_column = lax.axis_index("tp") * column_count
    moe_rows = moe_input.astype(jnp.float32)
    normed = (
        moe_rows
        * lax.rsqrt(jnp.mean(moe_rows * moe_rows, axis=1, keepdims=True) + norm_eps)
        * moe_gain
    ).astype(jnp.bfloat16)
    flat_routes = routes.reshape(-1)
    one_hot = (flat_routes[:, None] == jnp.arange(expert_count, dtype=jnp.int32)[None, :]).astype(
        jnp.int32
    )
    ranks = jnp.sum(jnp.cumsum(one_hot, axis=0) * one_hot, axis=1) - 1
    slot_index = flat_routes * capacity + ranks
    pair_token = jnp.arange(token_count * top_count, dtype=jnp.int32) // top_count
    slot_token = (
        jnp.full((expert_count * capacity,), token_count, jnp.int32).at[slot_index].set(pair_token)
    )
    padded = jnp.concatenate([normed, jnp.zeros((1, normed.shape[1]), jnp.bfloat16)], axis=0)
    outgoing = lax.dynamic_slice_in_dim(padded, first_column, column_count, 1)[slot_token]
    outgoing = outgoing.reshape(ep_count, local_experts, capacity, outgoing.shape[1])
    arrived = lax.all_to_all(outgoing, "ep", split_axis=0, concat_axis=0, tiled=True)
    arrived = lax.all_gather(arrived, "tp", axis=3, tiled=True)
    gate_val = jnp.einsum(
        "aecd,edf->aecf", arrived, expert_gate, preferred_element_type=jnp.float32
    )
    up_val = jnp.einsum("aecd,edf->aecf", arrived, expert_up, preferred_element_type=jnp.float32)
    hidden = (jax.nn.silu(gate_val) * up_val).astype(jnp.bfloat16)
    hidden = collect(hidden, "tp", 3)
    result = jnp.einsum(
        "aecf,efd->aecd", hidden, expert_down, preferred_element_type=jnp.float32
    ).astype(jnp.bfloat16)
    returned = lax.all_to_all(result, "ep", split_axis=0, concat_axis=0, tiled=True)
    picked = returned.reshape(expert_count * capacity, column_count)[slot_index]
    picked = picked.astype(jnp.float32).reshape(token_count, top_count, column_count)
    routed = jnp.sum(picked * route_weight[:, :, None], axis=1)
    shared_hidden = (
        jax.nn.silu(jnp.dot(normed, shared_gate, preferred_element_type=jnp.float32))
        * jnp.dot(normed, shared_up, preferred_element_type=jnp.float32)
    ).astype(jnp.bfloat16)
    mixer_sum = jnp.dot(
        lax.all_gather(heads_out, "tp", axis=1, tiled=True),
        out_weight,
        preferred_element_type=jnp.float32,
    )
    shared_all = lax.all_gather(shared_hidden, "tp", axis=1, tiled=True)
    moe_total = routed + jnp.dot(shared_all, shared_down, preferred_element_type=jnp.float32)
    return (mixer_sum.astype(jnp.bfloat16), moe_total.astype(jnp.bfloat16))


def solution(mesh):
    placed = (
        P("ep", "tp"),
        P("ep", "tp"),
        P("ep", "tp"),
        P("tp", None),
        P(None, "tp"),
        P("ep", None),
        P(),
        P("ep", None),
        P("ep", None),
        P("ep", None, "tp"),
        P("ep", None, "tp"),
        P("ep", None, "tp"),
        P(None, "tp"),
        P(None, "tp"),
        P(None, "tp"),
    )
    return jax.shard_map(
        local, mesh=mesh, in_specs=placed, out_specs=(P("ep", "tp"), P("ep", "tp")), check_vma=False
    )
```

profile of v0, /device:TPU:1, one launch (start us, length us, event | category | flops | bytes accessed | tf_op | source)
XLA Modules:
  0.0 554.8 jit_solution(1330439696241112962)
XLA Ops:
  11.6 4.1 scatter_custom_fusion
  16.0 2.9 gather_fusion
  19.3 40.2 %all_to_all.15 = bf16[32,4,9,128]{3,1,2,0:T(4,128)(2,1)S(1)} all-to-all(bf16[32,4,9,128]{3,1,2,0:T(4,128)(2,1)S(1)} %copy.46), channel_id=1, replica_groups=mesh['ep'=32,'tp'=16] {'ep'}, dimensions={0} | all-to-all | bytes 589824 | tf_op jit(solution)/shard_map/all_to_all | solution.py:130
  61.6 63.6 %all-gather.7.cloned.1.call-done = bf16[32,4,9,2048]{3,0,2,1:T(8,128)(2,1)} async-done(((bf16[32,4,9,128]{3,0,2,1:T(8,128)(2,1)}), bf16[32,4,9,2048]{3,0,2,1:T(8,128)(2,1)}) %all-gather.7.cloned.1.call-update) | async-done | bytes 4718608 | tf_op jit(solution)/shard_map/all_gather | solution.py:131
  125.2 3.8 convolution_bitcast_fusion.2
  130.5 3.2 broadcast_bitcast_fusion
  133.7 7.8 %reshape.164 = bf16[16,2,18432]{2,1,0:T(2,128)(2,1)} reshape(bf16[16,4,9,32,32]{4,3,2,1,0:T(8,128)(2,1)} %broadcast_bitcast_fusion) | data formatting | bytes 2359296
  141.5 4.8 all-to-all-start.1
  147.2 58.1 %all-gather.5.cloned.1.call-done = bf16[24576,128]{1,0:T(8,128)(2,1)} async-done(((bf16[768,128]{1,0:T(8,128)(2,1)}), bf16[24576,128]{1,0:T(8,128)(2,1)}) %all-gather.5.cloned.1.call-update) | async-done | bytes 6291472 | tf_op jit(solution)/shard_map/all_gather | solution.py:60
  205.4 76.2 %while.15 = (s32[]{:T(128)}, f32[1,768]{1,0:T(1,128)S(1)}, f32[1,768]{1,0:T(1,128)S(1)}, f32[1,768,64]{1,2,0:T(8,128)S(1)}, s32[48]{0:T(128)S(1)}, /*index=5*/s3...) while((s32[]{:T(128)}, f32[1,768]{1,0:T(1,128)S(1)}, ...), condition=%wide.region_5.6_spmd.clone, body=%wide.region_0.5_spmd.clone.sunk | while | flops 106270224 | bytes 5566899 | solution.py:99
  206.7 4.7 conditional.3
  209.6 1.4 fusion.4
  212.6 4.7 conditional.3
  215.5 1.4 fusion.4
  218.6 4.7 conditional.3
  282.3 3.8 reshape.165
  286.1 3.1 bitcast_bitcast_fusion
  289.2 7.6 %copy.48 = bf16[32,4,9,16,32]{4,3,0,2,1:T(8,128)(2,1)} copy(bf16[32,4,9,16,32]{4,0,2,1,3:T(8,128)(2,1)S(1)} %bitcast_bitcast_fusion) | data formatting | bytes 2359296 | tf_op jit(solution)/shard_map/transpose | solution.py:16
  296.8 6.5 %reshape.124 = bf16[32,4,9,512]{3,0,2,1:T(8,128)(2,1)S(1)} reshape(bf16[32,4,9,16,32]{4,3,0,2,1:T(8,128)(2,1)} %copy.48) | data formatting | bytes 2359296 | tf_op jit(solution)/shard_map/reshape | solution.py:16
  304.7 213.7 %all-to-all-start.2 = ((bf16[32,4,9,128]{3,1,2,0:T(4,128)(2,1)}), bf16[32,4,9,128]{3,1,2,0:T(4,128)(2,1)S(1)}, u32[]{:S(2)}, u32[]{:S(2)}) async-start(bf16[32,4,9,128]{3,1,2,0:T(4,128)(2,1)} %copy.49), calls=%async_computation.2 | async-start | bytes 589824 | tf_op jit(solution)/shard_map/all_to_all | solution.py:141
  519.2 20.5 %all_gather.15 = bf16[192,512]{0,1:T(8,128)(2,1)S(1)} all-gather(bf16[192,32]{0,1:T(8,128)(2,1)S(1)} %fusion.27), channel_id=1, replica_groups=mesh['ep'=32,'tp'=16] {'tp'}, dimensions={1}, use_global_device_ids=true | all-gather | bytes 208896 | tf_op jit(solution)/shard_map/all_gather | solution.py:154
  539.7 2.2 all-to-all-done.2
  542.2 1.9 gather_fusion.1
  545.5 2.7 fusion.22
  (252 shorter events, 51.7 us)
Async XLA Ops:
  7.2 296.1 %copy-start = (bf16[4,512,128]{2,1,0:T(8,128)(2,1)S(1)}, bf16[4,512,128]{2,1,0:T(8,128)(2,1)}, u32[]{:S(2)}) copy-start(bf16[4,512,128]{2,1,0:T(8,128)(2,1)} %param.30) | copy-start | bytes 1572868
  7.2 118.0 %all-gather.7.cloned.1.call-start = ((), (), s32[]{:S(2)}) async-start(), calls=%async_computation.4 | async-start | bytes 5013504 | tf_op jit(solution)/shard_map/all_gather | solution.py:131
  10.9 4.8 copy-start.1
  10.9 4.8 copy-start.8
  19.0 41.4 %copy-start.6 = (bf16[768,64]{0,1:T(8,128)(2,1)S(1)}, bf16[768,64]{0,1:T(8,128)(2,1)}, u32[]{:S(2)}) copy-start(bf16[768,64]{0,1:T(8,128)(2,1)} %param.20) | copy-start | bytes 294916
  19.0 41.6 %copy-start.7 = (bf16[768,64]{0,1:T(8,128)(2,1)S(1)}, bf16[768,64]{0,1:T(8,128)(2,1)}, u32[]{:S(2)}) copy-start(bf16[768,64]{0,1:T(8,128)(2,1)} %param.21) | copy-start | bytes 294916
  19.3 105.9 %copy-start.11 = (bf16[4,2048,32]{1,2,0:T(8,128)(2,1)S(1)}, bf16[4,2048,32]{1,2,0:T(8,128)(2,1)}, u32[]{:S(2)}) copy-start(bf16[4,2048,32]{1,2,0:T(8,128)(2,1)} %param.28) | copy-start | bytes 1572868
  60.3 145.0 %all-gather.5.cloned.1.call-start = ((), (), s32[]{:S(2)}) async-start(), calls=%async_computation.3 | async-start | bytes 6488064 | tf_op jit(solution)/shard_map/all_gather | solution.py:60
  61.6 67.5 %copy-start.12 = (bf16[4,2048,32]{1,2,0:T(8,128)(2,1)S(1)}, bf16[4,2048,32]{1,2,0:T(8,128)(2,1)}, u32[]{:S(2)}) copy-start(bf16[4,2048,32]{1,2,0:T(8,128)(2,1)} %param.29) | copy-start | bytes 1572868
  125.2 3.9 copy-start.10
  141.5 63.9 %copy-start.13 = (bf16[768,64]{0,1:T(8,128)(2,1)S(1)}, bf16[768,64]{0,1:T(8,128)(2,1)}, u32[]{:S(2)}) copy-start(bf16[768,64]{0,1:T(8,128)(2,1)} %param.19) | copy-start | bytes 294916
  141.5 140.8 %all-to-all-start.1 = ((bf16[16,2,18432]{2,1,0:T(2,128)(2,1)}), bf16[16,2,18432]{2,1,0:T(2,128)(2,1)S(1)}, u32[]{:S(2)}, u32[]{:S(2)}) async-start(bf16[16,2,18432]{2,1,0:T(2,128)(2,1)} %reshape.164), calls=%async_computation.1 | async-start | bytes 2359296 | tf_op jit(solution)/shard_map/all_to_all | solution.py:21
  146.3 399.2 %all-gather.9.cloned.1.call-start = ((), (), s32[]{:S(2)}) async-start(), calls=%async_computation.5 | async-start | bytes 1671168 | tf_op jit(solution)/shard_map/all_gather | solution.py:150
  303.3 215.1 %copy-start.9 = (f32[192,3]{0,1:T(4,128)S(1)}, f32[192,3]{0,1:T(4,128)}, u32[]{:S(2)}) copy-start(f32[192,3]{0,1:T(4,128)} %param.27) | copy-start | bytes 6916
  303.3 215.2 %copy-start.4 = (bf16[2048,32]{0,1:T(8,128)(2,1)S(1)}, bf16[2048,32]{0,1:T(8,128)(2,1)}, u32[]{:S(2)}) copy-start(bf16[2048,32]{0,1:T(8,128)(2,1)} %param.31) | copy-start | bytes 393220
  303.8 215.1 %copy-start.5 = (bf16[2048,32]{0,1:T(8,128)(2,1)S(1)}, bf16[2048,32]{0,1:T(8,128)(2,1)}, u32[]{:S(2)}) copy-start(bf16[2048,32]{0,1:T(8,128)(2,1)} %param.32) | copy-start | bytes 393220
  304.7 237.3 %all-to-all-start.2 = ((bf16[32,4,9,128]{3,1,2,0:T(4,128)(2,1)}), bf16[32,4,9,128]{3,1,2,0:T(4,128)(2,1)S(1)}, u32[]{:S(2)}, u32[]{:S(2)}) async-start(bf16[32,4,9,128]{3,1,2,0:T(4,128)(2,1)} %copy.49), calls=%async_computation.2 | async-start | bytes 589824 | tf_op jit(solution)/shard_map/all_to_all | solution.py:141
  542.1 2.6 copy-start.3
  542.2 3.3 copy-start.2
Sparse Core Ops, SparseCore 0:
  60.4 64.7 all-gather.6
  127.9 77.4 all-gather.4
  282.4 260.1 all-gather.8
where the time goes:
time: 559 us; the launch traced here: 555 us
  starting transfers between devices  219 us (39%)
  waiting for transfers between devices  124 us (22%)
  local copies, waits for them, and re-layouts  76.5 us (14%)
  blocking collectives  60.7 us (11%)
  loops' own time  36.1 us (6%)
  matrix products  18.3 us (3%)
  between operations  14.2 us (3%)
  other arithmetic  6.13 us (1%)
    all_to_all x1, starting transfers between devices, local(): lax.all_to_all(result, 'ep', split_axis=0, concat_axis=0, tiled=True)  214 us
    all_gather x1, waiting for transfers between devices, local(): arrived = lax.all_gather(arrived, 'tp', axis=3, tiled=True)  63.6 us
    all_gather x1, waiting for transfers between devices, local(): shard_rows = lax.all_gather(key_value, 'ep', axis=0, tiled=True)  58.1 us
    all_to_all x1, blocking collectives, local(): lax.all_to_all(outgoing, 'ep', split_axis=0, concat_axis=0, tiled=True)  40.2 us
    another operation x1, loops' own time, local(): lax.scan(one_span, initial, jnp.arange(piece_len // key_span, dtype=jnp.i...  33.2 us
    dynamic_slice x48, local copies, waits for them, and re-layouts, local(): lax.scan(one_span, initial, jnp.arange(piece_len // key_span, dtype=jnp.i...  28.1 us
    all_gather x1, blocking collectives, local(): shared_all = lax.all_gather(shared_hidden, 'tp', axis=1, tiled=True)  20.5 us
    unnamed x35, local copies, waits for them, and re-layouts  16.1 us
  transfers between devices with their start and end apart: 5, of which 3 were waited for; matrix products, arithmetic and copies ran while one was open for 15% of the time, Pallas kernels for 0%

commit v1 on v0

v1 whole, which is shorter than its diff:
```python
import jax
import jax.numpy as jnp
from jax import lax
from jax.experimental import pallas as pl
from jax.experimental.pallas import tpu as pltpu
from jax.sharding import PartitionSpec as P

HEAD = 64


neg_fill = -1e30
norm_eps = 1e-06


def joined_along(pieces, dim):
    dims = list(pieces.shape[1:])
    dims[dim] *= pieces.shape[0]
    return jnp.moveaxis(pieces, 0, dim).reshape(dims)


def sent_to_all(array, axis):
    copies = jnp.broadcast_to(array, (lax.axis_size(axis), *array.shape))
    return lax.all_to_all(copies, axis, split_axis=0, concat_axis=0, tiled=True)


def collect(array, axis, dim):
    return joined_along(sent_to_all(array, axis), dim)


MESH = pl.DeviceIdType.MESH
SPAN = 768
Z = 16
TP = 16
UP = 8
DOWN = 7


def remote(src, dst, send, recv, ep, tp):
    return pltpu.make_async_remote_copy(
        src_ref=src, dst_ref=dst, send_sem=send, recv_sem=recv, device_id=(ep, tp), device_id_type=MESH
    )


def attention_kernel(
    q_ref,
    k_hbm,
    v_hbm,
    gate_ref,
    wo_ref,
    out_ref,
    kbuf,
    vbuf,
    q_scr,
    m_scr,
    acc,
    packed,
    heads,
    wide,
    own_sem,
    up_send,
    up_recv,
    dn_send,
    dn_recv,
    pr_send,
    pr_recv,
    hd_send,
    hd_recv,
):
    ep = lax.axis_index("ep")
    tp = lax.axis_index("tp")
    z = ep // 2
    c = ep % 2
    above = ((z + 1) % Z) * 2 + c
    below = ((z + Z - 1) % Z) * 2 + c
    partner = z * 2 + (1 - c)

    own = [
        pltpu.make_async_copy(k_hbm, kbuf.at[ep], own_sem.at[0]),
        pltpu.make_async_copy(v_hbm, vbuf.at[ep, pl.ds(64, 64)], own_sem.at[1]),
    ]
    for copy in own:
        copy.start()

    barrier = pltpu.get_barrier_semaphore()
    for peer in (above, below, partner):
        pl.semaphore_signal(barrier, inc=1, device_id=(peer, tp), device_id_type=MESH)
    for hop in range(1, TP):
        pl.semaphore_signal(
            barrier, inc=1, device_id=(ep, (tp + hop) % TP), device_id_type=MESH
        )

    def part(block, half):
        return kbuf.at[block] if half == 0 else vbuf.at[block, pl.ds(64, 64)]

    def up_copy(step, half):
        block = ((z - step + Z) % Z) * 2 + c
        return remote(
            part(block, half), part(block, half), up_send.at[step, half], up_recv.at[step, half], above, tp
        )

    def dn_copy(step, half):
        block = ((z + step) % Z) * 2 + c
        return remote(
            part(block, half), part(block, half), dn_send.at[step, half], dn_recv.at[step, half], below, tp
        )

    def up_landed(step, half):
        block = ((z - step + Z) % Z) * 2 + c
        return remote(
            part(block, half), part(block, half), up_send.at[step - 1, half], up_recv.at[step - 1, half], below, tp
        )

    def dn_landed(step, half):
        block = ((z + step) % Z) * 2 + c
        return remote(
            part(block, half), part(block, half), dn_send.at[step - 1, half], dn_recv.at[step - 1, half], above, tp
        )

    def pr_copy(slot, block, half):
        return remote(
            part(block, half), part(block, half), pr_send.at[slot, half], pr_recv.at[slot, half], partner, tp
        )

    def up_sends(step):
        return (z - step >= 0) & (z < Z - 1)

    def up_lands(step):
        return z - step >= 0

    def dn_moves(step):
        return (z + step) % Z <= 6

    def dn_used(step):
        return ((z + step) % Z <= 6) & ((z + step) % Z < z)

    vbuf[:, 0:64, :] = jnp.ones((2 * Z, 64, SPAN), jnp.bfloat16)
    q_scr[...] = (q_ref[...].astype(jnp.float32) * 0.125).T.astype(jnp.bfloat16)
    m_scr[...] = jnp.full(m_scr.shape, -1e30, jnp.float32)
    acc[...] = jnp.zeros(acc.shape, jnp.float32)

    for copy in own:
        copy.wait()
    pl.semaphore_wait(barrier, TP + 2)

    for half in range(2):

        @pl.when(up_sends(0))
        def _():
            up_copy(0, half).start()

        @pl.when(dn_moves(0))
        def _():
            dn_copy(0, half).start()

        @pl.when(c == 0)
        def _():
            pr_copy(0, ep, half).start()

    gate_first = gate_ref[:, pl.ds(pl.multiple_of(ep * SPAN, 128), 128)][:, 0:1]

    def attend(block, diagonal):
        bias = gate_first - gate_ref[:, pl.ds(pl.multiple_of(block * SPAN, 128), SPAN)]
        keys = kbuf[block]
        values = vbuf[block]
        rows = 256
        for start in range(0, SPAN, rows):
            span = pl.ds(start, rows)
            scores = jnp.dot(q_scr[span, :], keys, preferred_element_type=jnp.float32) + bias
            if diagonal:
                row = lax.broadcasted_iota(jnp.int32, scores.shape, 0) + start
                column = lax.broadcasted_iota(jnp.int32, scores.shape, 1)
                scores = jnp.where(column <= row, scores, -1e30)
            old = m_scr[span, :]
            new = jnp.maximum(old, jnp.max(scores, axis=1, keepdims=True))
            probs = jnp.exp(scores - jnp.concatenate([new] * (SPAN // 128), axis=1))
            summed = lax.dot_general(
                probs.astype(jnp.bfloat16),
                values,
                (((1,), (1,)), ((), ())),
                preferred_element_type=jnp.float32,
            )
            acc[span, :] = acc[span, :] * jnp.exp(old - new) + summed
            m_scr[span, :] = new

    attend(ep, True)

    def ring(step, carry):
        up_ok = up_lands(step)
        dn_ok = (step <= DOWN) & dn_moves(step)
        for half in range(2):

            @pl.when(up_ok)
            def _():
                up_landed(step, half).wait_recv()

                @pl.when((step < UP) & up_sends(step))
                def _():
                    up_copy(step, half).start()

                pr_copy(step, ((z - step + Z) % Z) * 2 + c, half).start()

            @pl.when(dn_ok)
            def _():
                dn_landed(step, half).wait_recv()

                @pl.when(step < DOWN)
                def _():
                    dn_copy(step, half).start()

                @pl.when(dn_used(step))
                def _():
                    pr_copy(UP + step, ((z + step) % Z) * 2 + c, half).start()

        def one(i, carry):
            down = i % 2
            other = i // 2
            used = jnp.where(
                down == 1, ((step <= DOWN) & dn_used(step)).astype(jnp.int32), up_ok.astype(jnp.int32)
            )
            origin = jnp.where(down == 1, (z + step) % Z, (z - step + Z) % Z)
            block = origin * 2 + jnp.where(other == 1, 1 - c, c)

            @pl.when(used == 1)
            def _():
                @pl.when(other == 1)
                def _():
                    slot = step + down * UP
                    for half in range(2):
                        pr_copy(slot, block, half).wait_recv()

                attend(block, False)

            return carry

        lax.fori_loop(0, 4, one, 0)
        return carry

    @pl.when(c == 1)
    def _():
        for half in range(2):
            pr_copy(0, partner, half).wait_recv()
        attend(partner, False)

    lax.fori_loop(1, UP + 1, ring, 0)

    total = acc[...]
    ratio = total / pltpu.roll(total, 64, 1)
    lane = lax.broadcasted_iota(jnp.int32, (384, 128), 1)
    packed[...] = jnp.where(lane < 64, pltpu.roll(ratio[:384], 64, 1), ratio[384:]).astype(jnp.bfloat16)

    def head_copy(hop):
        return remote(
            packed, heads.at[tp], hd_send.at[hop], hd_recv.at[tp], ep, (tp + hop) % TP
        )

    for hop in range(1, TP):
        head_copy(hop).start()
    heads[tp] = packed[...]
    for head in range(TP):
        w = wo_ref[head * 64 : head * 64 + 64, :]
        wide[head * 128 : head * 128 + 64, :] = jnp.concatenate([w, jnp.zeros_like(w)], axis=1)
        wide[head * 128 + 64 : head * 128 + 128, :] = jnp.concatenate([jnp.zeros_like(w), w], axis=1)
    for hop in range(1, TP):
        source = (tp + TP - hop) % TP
        remote(
            packed, heads.at[source], hd_send.at[hop], hd_recv.at[source], ep, source
        ).wait_recv()
    mixed = jnp.zeros((384, 256), jnp.float32)
    for head in range(TP):
        mixed = mixed + jnp.dot(
            heads[head], wide[head * 128 : head * 128 + 128, :], preferred_element_type=jnp.float32
        )
    out_ref[0:384, :] = mixed[:, 0:128].astype(jnp.bfloat16)
    out_ref[384:768, :] = mixed[:, 128:256].astype(jnp.bfloat16)

    for hop in range(1, TP):
        head_copy(hop).wait_send()

    def drain(step, carry):
        for half in range(2):

            @pl.when(up_sends(step) & (step < UP))
            def _():
                up_copy(step, half).wait_send()

            @pl.when((step < DOWN) & dn_moves(step))
            def _():
                dn_copy(step, half).wait_send()

            @pl.when((step >= 1) & up_lands(step))
            def _():
                pr_copy(step, ((z - step + Z) % Z) * 2 + c, half).wait_send()

            @pl.when((step >= 1) & (step <= DOWN) & dn_used(step))
            def _():
                pr_copy(UP + step, ((z + step) % Z) * 2 + c, half).wait_send()

        return carry

    @pl.when(c == 0)
    def _():
        for half in range(2):
            pr_copy(0, ep, half).wait_send()

    lax.fori_loop(0, UP + 1, drain, 0)


def attention(query_rows, key_rows, value_rows, cum_gate, out_weight):
    vmem = pl.BlockSpec(memory_space=pltpu.VMEM)
    hbm = pl.BlockSpec(memory_space=pl.ANY)
    dma = pltpu.SemaphoreType.DMA
    return pl.pallas_call(
        attention_kernel,
        out_shape=jax.ShapeDtypeStruct((SPAN, 128), jnp.bfloat16),
        in_specs=[vmem, hbm, hbm, vmem, vmem],
        out_specs=vmem,
        scratch_shapes=[
            pltpu.VMEM((2 * Z, 64, SPAN), jnp.bfloat16),
            pltpu.VMEM((2 * Z, 128, SPAN), jnp.bfloat16),
            pltpu.VMEM((SPAN, 64), jnp.bfloat16),
            pltpu.VMEM((SPAN, 128), jnp.float32),
            pltpu.VMEM((SPAN, 128), jnp.float32),
            pltpu.VMEM((384, 128), jnp.bfloat16),
            pltpu.VMEM((TP, 384, 128), jnp.bfloat16),
            pltpu.VMEM((TP * 128, 256), jnp.bfloat16),
            dma((2,)),
            dma((UP, 2)),
            dma((UP, 2)),
            dma((DOWN, 2)),
            dma((DOWN, 2)),
            dma((UP + DOWN + 1, 2)),
            dma((UP + DOWN + 1, 2)),
            dma((TP,)),
            dma((TP,)),
        ],
        compiler_params=pltpu.CompilerParams(
            collective_id=0, has_side_effects=True, vmem_limit_bytes=56 * 2**20
        ),
        cost_estimate=pl.CostEstimate(flops=5 * 10**10, bytes_accessed=10**7, transcendentals=0),
        name="attention",
    )(query_rows.T, key_rows.T, value_rows.T, cum_gate, out_weight)


def local(
    query_rows,
    key_rows,
    value_rows,
    cum_gate,
    out_weight,
    moe_input,
    moe_gain,
    routes,
    route_weight,
    expert_gate,
    expert_up,
    expert_down,
    shared_gate,
    shared_up,
    shared_down,
):
    mixer_out = attention(query_rows, key_rows, value_rows, cum_gate, out_weight)
    token_count = moe_input.shape[0]
    top_count = routes.shape[1]
    local_experts = expert_gate.shape[0]
    ep_count = lax.axis_size("ep")
    expert_count = local_experts * ep_count
    capacity = 2 * token_count * top_count // expert_count
    column_count = expert_down.shape[2]
    first_column = lax.axis_index("tp") * column_count
    moe_rows = moe_input.astype(jnp.float32)
    normed = (
        moe_rows
        * lax.rsqrt(jnp.mean(moe_rows * moe_rows, axis=1, keepdims=True) + norm_eps)
        * moe_gain
    ).astype(jnp.bfloat16)
    flat_routes = routes.reshape(-1)
    one_hot = (flat_routes[:, None] == jnp.arange(expert_count, dtype=jnp.int32)[None, :]).astype(
        jnp.int32
    )
    ranks = jnp.sum(jnp.cumsum(one_hot, axis=0) * one_hot, axis=1) - 1
    slot_index = flat_routes * capacity + ranks
    pair_token = jnp.arange(token_count * top_count, dtype=jnp.int32) // top_count
    slot_token = (
        jnp.full((expert_count * capacity,), token_count, jnp.int32).at[slot_index].set(pair_token)
    )
    padded = jnp.concatenate([normed, jnp.zeros((1, normed.shape[1]), jnp.bfloat16)], axis=0)
    outgoing = lax.dynamic_slice_in_dim(padded, first_column, column_count, 1)[slot_token]
    outgoing = outgoing.reshape(ep_count, local_experts, capacity, outgoing.shape[1])
    arrived = lax.all_to_all(outgoing, "ep", split_axis=0, concat_axis=0, tiled=True)
    arrived = lax.all_gather(arrived, "tp", axis=3, tiled=True)
    gate_val = jnp.einsum(
        "aecd,edf->aecf", arrived, expert_gate, preferred_element_type=jnp.float32
    )
    up_val = jnp.einsum("aecd,edf->aecf", arrived, expert_up, preferred_element_type=jnp.float32)
    hidden = (jax.nn.silu(gate_val) * up_val).astype(jnp.bfloat16)
    hidden = collect(hidden, "tp", 3)
    result = jnp.einsum(
        "aecf,efd->aecd", hidden, expert_down, preferred_element_type=jnp.float32
    ).astype(jnp.bfloat16)
    returned = lax.all_to_all(result, "ep", split_axis=0, concat_axis=0, tiled=True)
    picked = returned.reshape(expert_count * capacity, column_count)[slot_index]
    picked = picked.astype(jnp.float32).reshape(token_count, top_count, column_count)
    routed = jnp.sum(picked * route_weight[:, :, None], axis=1)
    shared_hidden = (
        jax.nn.silu(jnp.dot(normed, shared_gate, preferred_element_type=jnp.float32))
        * jnp.dot(normed, shared_up, preferred_element_type=jnp.float32)
    ).astype(jnp.bfloat16)
    shared_all = lax.all_gather(shared_hidden, "tp", axis=1, tiled=True)
    moe_total = routed + jnp.dot(shared_all, shared_down, preferred_element_type=jnp.float32)
    return (mixer_out, moe_total.astype(jnp.bfloat16))


def solution(mesh):
    placed = (
        P("ep", "tp"),
        P("ep", "tp"),
        P("ep", "tp"),
        P("tp", None),
        P(None, "tp"),
        P("ep", None),
        P(),
        P("ep", None),
        P("ep", None),
        P("ep", None, "tp"),
        P("ep", None, "tp"),
        P("ep", None, "tp"),
        P(None, "tp"),
        P(None, "tp"),
        P(None, "tp"),
    )
    return jax.shard_map(
        local, mesh=mesh, in_specs=placed, out_specs=(P("ep", "tp"), P("ep", "tp")), check_vma=False
    )
```

time: 559 us -> 318 us (0.57)
  the two profiles are of different devices: /device:TPU:1 before, /device:TPU:416 now
where the time goes in v1:
time: 318 us; the launch traced here: 317 us
  Pallas kernels  86.3 us (27%)
  blocking collectives  73.3 us (23%)
  waiting for transfers between devices  73 us (23%)
  local copies, waits for them, and re-layouts  47.7 us (15%)
  between operations  14.5 us (5%)
  starting transfers between devices  11.8 us (4%)
  matrix products  7.28 us (2%)
  other arithmetic  3.47 us (1%)
    pallas_call x1, Pallas kernels, attention(): pl.pallas_call(attention_kernel, out_shape=jax.ShapeDtypeStruct((SPAN, 12...  86.3 us
    all_gather x1, waiting for transfers between devices, local(): arrived = lax.all_gather(arrived, 'tp', axis=3, tiled=True)  73 us
    all_to_all x1, blocking collectives, local(): lax.all_to_all(outgoing, 'ep', split_axis=0, concat_axis=0, tiled=True)  27.8 us
    all_gather x1, blocking collectives, local(): shared_all = lax.all_gather(shared_hidden, 'tp', axis=1, tiled=True)  23 us
    all_to_all x1, blocking collectives, sent_to_all(): return lax.all_to_all(copies, axis, split_axis=0, concat_axis=0, tiled=True)  22.5 us
    unnamed x28, local copies, waits for them, and re-layouts  18.7 us
    all_to_all x1, starting transfers between devices, local(): lax.all_to_all(result, 'ep', split_axis=0, concat_axis=0, tiled=True)  11.8 us
    transpose x2, local copies, waits for them, and re-layouts, joined_along(): return jnp.moveaxis(pieces, 0, dim).reshape(dims)  10.7 us
  transfers between devices with their start and end apart: 2, of which 1 were waited for; matrix products, arithmetic and copies ran while one was open for 0% of the time, Pallas kernels for 27%

profile of v1, /device:TPU:416, one launch (start us, length us, event | category | flops | bytes accessed | tf_op | source)
XLA Modules:
  0.0 317.2 jit_solution(4911036661886078260)
XLA Ops:
  7.3 0.8 broadcast_multiply_fusion
  8.0 0.8 copy.34
  8.9 1.4 fusion
  11.6 4.1 %scatter_custom_fusion = s32[1152]{0:T(1024)S(1)} fusion(s32[576]{0:T(1024)S(1)} %fusion.19, s32[576]{0:T(1024)S(1)} %add_select_fusion, s32[]{:T(128)} %constant.25.clone.1), kind=kCustom, calls=%fused_computation.42 | custom fusion | bytes 4612 | tf_op jit(solution)/shard_map/scatter | solution.py:384
  16.1 2.9 gather_fusion
  19.3 27.8 %all_to_all.15 = bf16[32,4,9,128]{3,1,2,0:T(4,128)(2,1)S(1)} all-to-all(bf16[32,4,9,128]{3,1,2,0:T(4,128)(2,1)S(1)} %copy.37), channel_id=1, replica_groups=mesh['ep'=32,'tp'=16] {'ep'}, dimensions={0} | all-to-all | bytes 589824 | tf_op jit(solution)/shard_map/all_to_all | solution.py:389
  47.1 0.8 copy.38
  47.9 73.0 %all-gather.2.cloned.1.call-done = bf16[32,4,9,2048]{3,0,2,1:T(8,128)(2,1)} async-done(((bf16[32,4,9,128]{3,0,2,1:T(8,128)(2,1)}), bf16[32,4,9,2048]{3,0,2,1:T(8,128)(2,1)}) %all-gather.2.cloned.1.call-update) | async-done | bytes 4718608 | tf_op jit(solution)/shard_map/all_gather | solution.py:390
  120.9 3.8 %convolution_bitcast_fusion.1 = f32[32,4,9,32]{3,0,2,1:T(8,128)S(1)} fusion(bf16[32,4,9,2048]{3,0,2,1:T(8,128)(2,1)} %all-gather.2.cloned.1.call-done, bf16[4,2048,32]{1,2,0:T(8,128)(2,1)S(1)} %copy-done.9), kind=kOutput, calls=%fused_computation.10 | convolution fusion | flops 150994944 | bytes 5390336 | tf_op jit(solution)/shard_map/aecd,edf->aecf/dot_general | solution.py:391
  124.8 1.4 fusion.4
  126.2 3.1 broadcast_bitcast_fusion
  129.3 7.0 %reshape.111 = bf16[16,2,18432]{2,1,0:T(2,128)(2,1)S(1)} reshape(bf16[16,4,9,32,32]{4,3,2,1,0:T(8,128)(2,1)} %broadcast_bitcast_fusion) | data formatting | bytes 2359296
  136.3 22.5 %all_to_all.16 = bf16[16,2,18432]{2,1,0:T(2,128)(2,1)} all-to-all(bf16[16,2,18432]{2,1,0:T(2,128)(2,1)S(1)} %reshape.111), channel_id=1, replica_groups=mesh['ep'=32,'tp'=16] {'tp'}, dimensions={0} | all-to-all | bytes 2359296 | tf_op jit(solution)/shard_map/all_to_all | solution.py:23
  158.8 6.8 %reshape.112 = bf16[16,4,9,32,32]{4,3,2,1,0:T(8,128)(2,1)} reshape(bf16[16,2,18432]{2,1,0:T(2,128)(2,1)} %all_to_all.16) | data formatting | bytes 2359296
  165.6 3.1 bitcast_bitcast_fusion
  168.8 7.6 %copy.39 = bf16[32,4,9,16,32]{4,3,0,2,1:T(8,128)(2,1)} copy(bf16[32,4,9,16,32]{4,0,2,1,3:T(8,128)(2,1)S(1)} %bitcast_bitcast_fusion) | data formatting | bytes 2359296 | tf_op jit(solution)/shard_map/transpose | solution.py:18
  176.3 6.5 %reshape.76 = bf16[32,4,9,512]{3,0,2,1:T(8,128)(2,1)S(1)} reshape(bf16[32,4,9,16,32]{4,3,0,2,1:T(8,128)(2,1)} %copy.39) | data formatting | bytes 2359296 | tf_op jit(solution)/shard_map/reshape | solution.py:18
  183.3 0.9 copy.40
  184.2 11.8 %all-to-all-start.2 = ((bf16[32,4,9,128]{3,1,2,0:T(4,128)(2,1)}), bf16[32,4,9,128]{3,1,2,0:T(4,128)(2,1)S(1)}, u32[]{:S(2)}, u32[]{:S(2)}) async-start(bf16[32,4,9,128]{3,1,2,0:T(4,128)(2,1)} %copy.40), calls=%async_computation.2 | async-start | bytes 589824 | tf_op jit(solution)/shard_map/all_to_all | solution.py:400
  196.0 86.3 %attention.1 = bf16[768,128]{1,0:T(8,128)(2,1)} custom-call(bf16[64,768]{1,0:T(8,128)(2,1)} %bitcast.58, bf16[64,768]{1,0:T(8,128)(2,1)} %bitcast.59, bf16[64,768]{1,0:T(8,128)(2,1)} %bitcast.60, f32[1,24576]{1,0:T(1,128)} %gate_ref.1, bf16[1024,128]{1,0:T(8,128)(2,1)} %wo_ref.1), custom_call_target="tpu_custom_call" | custom-call | flops 49999998976 | bytes 10000000 | tf_op jit(solution)/shard_map/attention/pallas_call | solution.py:312
  283.2 23.0 %all_gather.7 = bf16[192,512]{0,1:T(8,128)(2,1)S(1)} all-gather(bf16[192,32]{0,1:T(8,128)(2,1)S(1)} %fusion.7), channel_id=1, replica_groups=mesh['ep'=32,'tp'=16] {'tp'}, dimensions={1}, use_global_device_ids=true | all-gather | bytes 208896 | tf_op jit(solution)/shard_map/all_gather | solution.py:408
  306.4 1.9 gather_fusion.1
  308.8 0.9 fusion.6
  309.7 0.7 copy.49
  (55 shorter events, 4.0 us)
Async XLA Ops:
  7.2 175.7 %copy-start = (bf16[4,512,128]{2,1,0:T(8,128)(2,1)S(1)}, bf16[4,512,128]{2,1,0:T(8,128)(2,1)}, u32[]{:S(2)}) copy-start(bf16[4,512,128]{2,1,0:T(8,128)(2,1)} %param.26) | copy-start | bytes 1572868
  7.2 8.6 %copy-start.1 = (bf16[192,2048]{1,0:T(8,128)(2,1)S(1)}, bf16[192,2048]{1,0:T(8,128)(2,1)}, u32[]{:S(2)}) copy-start(bf16[192,2048]{1,0:T(8,128)(2,1)} %param.20) | copy-start | bytes 2359300
  7.2 8.6 %copy-start.6 = (f32[2048]{0:T(1024)S(1)}, f32[2048]{0:T(1024)}, u32[]{:S(2)}) copy-start(f32[2048]{0:T(1024)} %param.21) | copy-start | bytes 24580
  7.2 113.7 %all-gather.2.cloned.1.call-start = ((), (), s32[]{:S(2)}) async-start(), calls=%async_computation.3 | async-start | bytes 5013504 | tf_op jit(solution)/shard_map/all_gather | solution.py:390
  11.3 109.6 %copy-start.9 = (bf16[4,2048,32]{1,2,0:T(8,128)(2,1)S(1)}, bf16[4,2048,32]{1,2,0:T(8,128)(2,1)}, u32[]{:S(2)}) copy-start(bf16[4,2048,32]{1,2,0:T(8,128)(2,1)} %param.24) | copy-start | bytes 1572868
  47.9 76.8 %copy-start.10 = (bf16[4,2048,32]{1,2,0:T(8,128)(2,1)S(1)}, bf16[4,2048,32]{1,2,0:T(8,128)(2,1)}, u32[]{:S(2)}) copy-start(bf16[4,2048,32]{1,2,0:T(8,128)(2,1)} %param.25) | copy-start | bytes 1572868
  120.9 3.9 %copy-start.8 = (bf16[32,4,9,2048]{3,0,2,1:T(8,128)(2,1)S(1)}, bf16[32,4,9,2048]{3,0,2,1:T(8,128)(2,1)}, u32[]{:S(2)}) copy-start(bf16[32,4,9,2048]{3,0,2,1:T(8,128)(2,1)} %all-gather.2.cloned.1.call-done) | copy-start | bytes 14155780
  184.2 122.0 %all-to-all-start.2 = ((bf16[32,4,9,128]{3,1,2,0:T(4,128)(2,1)}), bf16[32,4,9,128]{3,1,2,0:T(4,128)(2,1)S(1)}, u32[]{:S(2)}, u32[]{:S(2)}) async-start(bf16[32,4,9,128]{3,1,2,0:T(4,128)(2,1)} %copy.40), calls=%async_computation.2 | async-start | bytes 589824 | tf_op jit(solution)/shard_map/all_to_all | solution.py:400
  195.9 86.3 %copy-start.7 = (f32[192,3]{0,1:T(4,128)S(1)}, f32[192,3]{0,1:T(4,128)}, u32[]{:S(2)}) copy-start(f32[192,3]{0,1:T(4,128)} %param.23) | copy-start | bytes 6916
  196.0 86.5 %copy-start.4 = (bf16[2048,32]{0,1:T(8,128)(2,1)S(1)}, bf16[2048,32]{0,1:T(8,128)(2,1)}, u32[]{:S(2)}) copy-start(bf16[2048,32]{0,1:T(8,128)(2,1)} %param.27) | copy-start | bytes 393220
  196.0 86.8 %copy-start.5 = (bf16[2048,32]{0,1:T(8,128)(2,1)S(1)}, bf16[2048,32]{0,1:T(8,128)(2,1)}, u32[]{:S(2)}) copy-start(bf16[2048,32]{0,1:T(8,128)(2,1)} %param.28) | copy-start | bytes 393220
  282.3 26.5 %copy-start.3 = (bf16[512,128]{1,0:T(8,128)(2,1)S(1)}, bf16[512,128]{1,0:T(8,128)(2,1)}, u32[]{:S(2)}) copy-start(bf16[512,128]{1,0:T(8,128)(2,1)} %param.29) | copy-start | bytes 393220
  282.3 27.4 %copy-start.2 = (bf16[768,128]{1,0:T(8,128)(2,1)S(1)}, bf16[768,128]{1,0:T(8,128)(2,1)}, u32[]{:S(2)}) copy-start(bf16[768,128]{1,0:T(8,128)(2,1)} %attention.1) | copy-start | bytes 589828
Sparse Core Ops, SparseCore 0:
  48.0 72.8 all-gather.1
